TPU v7x, 32 devices: a whole 2x2x4 slice. The times are simulated.
32 devices in a mesh: sp: 8 (over z, x), tp: 4 (over y, core).
Axes of the slice: x: 2, y: 2, z: 4, core: 2. Of those that a mesh axis runs over, the one named last changes fastest.
Arguments:
- queries: bfloat16 [2048, 1024], P('sp', 'tp'), may hold values from -6 to 6
- keys: bfloat16 [2048, 256], P('sp'), may hold values from -6 to 6
- values: bfloat16 [2048, 256], P('sp'), may hold values from -6 to 6
- sink: float32 [16], P('tp'), may hold values from 3 to 6
- w_out: bfloat16 [1024, 2048], P('tp'), may hold values from -0.1875 to 0.1875
- stream: bfloat16 [2048, 2048], P(('sp', 'tp')), may hold values from -6 to 6
- gain: bfloat16 [2048], replicated, may hold values from 0.099609375 to 1.8984375
- routes: int32 [2048, 4], P('sp'), may hold values from 0 to 63, all different within a row; in each aligned block of 64 rows (0 to 63, 64 to 127, ...) at most 8 rows name the same one
- route_weights: float32 [2048, 4], P('sp'), may hold values from 0.2 to 1
- w_gate: bfloat16 [64, 1024, 2048], P('sp', 'tp'), may hold values from -0.125 to 0.125
- w_up: bfloat16 [64, 1024, 2048], P('sp', 'tp'), may hold values from -0.125 to 0.125
- w_down: bfloat16 [64, 1024, 2048], P('sp', None, 'tp'), may hold values from -0.1875 to 0.1875
- shared_gate: bfloat16 [1024, 2048], P('tp'), may hold values from -0.125 to 0.125
- shared_up: bfloat16 [1024, 2048], P('tp'), may hold values from -0.125 to 0.125
- shared_down: bfloat16 [1024, 2048], P(None, 'tp'), may hold values from -0.1875 to 0.1875
Outputs:
- layer_out: bfloat16 [2048, 2048], P('sp', 'tp')
Inputs may be any that keep to these rules, and one draw needn't show every extreme that they name: `routes`: in each aligned block of 64 rows no expert is named in more than 8 rows, and some blocks reach 8; a row names 4 different experts.
All inputs are finite; a program needn't handle non-finite values.
Results may differ from a plain program's by a relative error of at most 0.014.
Values may be sent and summed in bfloat16 or wider, within the bound.
A program may use at most 128 MiB of HBM per device.

v0:
```python
import jax
import jax.numpy as jnp
from jax import lax
from jax.sharding import PartitionSpec as P

D = 2048
HEADS = 16
KV_HEADS = 4
HD = 64
WINDOW = 128
EXPERTS = 64
TOPK = 4
NORM_EPS = 1e-05


def with_halo(array, sides, width):
    for axis, dim in sides:
        devices, length = (lax.axis_size(axis), array.shape[dim])
        up = [(i, (i + 1) % devices) for i in range(devices - 1)]
        down = [(j, i) for i, j in up]
        last = lax.slice_in_dim(array, length - width, length, axis=dim)
        leading = lax.slice_in_dim(array, 0, width, axis=dim)
        before = lax.ppermute(last, axis, up)
        after = lax.ppermute(leading, axis, down)
        array = jnp.concatenate([before, array, after], axis=dim)
    return array


def slot_ids(block_routes, capacity):
    flat_routes = block_routes.reshape(-1)
    hit_table = (flat_routes[:, None] == jnp.arange(EXPERTS)[None, :]).astype(jnp.int32)
    earlier = jnp.cumsum(hit_table, axis=0) - hit_table
    slot_rank = jnp.sum(earlier * hit_table, axis=1)
    return flat_routes * capacity + slot_rank


def local(
    queries,
    keys,
    values,
    sink,
    w_out,
    stream,
    gain,
    routes,
    route_weights,
    w_gate,
    w_up,
    w_down,
    shared_gate,
    shared_up,
    shared_down,
):
    tok_dev = queries.shape[0]
    n_tp = lax.axis_size("tp")
    n_sp = lax.axis_size("sp")
    tp_idx = lax.axis_index("tp")
    sp_idx = lax.axis_index("sp")
    heads_dev = HEADS // n_tp
    group = HEADS // KV_HEADS
    kv_head = tp_idx * heads_dev // group
    key_own = lax.dynamic_slice_in_dim(keys, kv_head * HD, HD, 1)
    value_own = lax.dynamic_slice_in_dim(values, kv_head * HD, HD, 1)
    paired = jnp.concatenate([key_own, value_own], axis=1)
    padded = with_halo(paired, (("sp", 0),), WINDOW)
    blocks = tok_dev // WINDOW
    framed = padded.reshape(blocks + 2, WINDOW, 2 * HD)
    banded = jnp.concatenate([framed[:-2], framed[1:-1], framed[2:]], axis=1)
    key_band = banded[:, :, :HD]
    value_band = banded[:, :, HD:]
    query_blocks = queries.reshape(blocks, WINDOW, heads_dev, HD)
    scores = jnp.einsum(
        "nqhd,njd->nhqj", query_blocks, key_band, preferred_element_type=jnp.float32
    ) * HD ** (-0.5)
    offset = sp_idx * tok_dev
    seq_total = tok_dev * n_sp
    query_pos = (
        offset + jnp.arange(blocks)[:, None, None] * WINDOW + jnp.arange(WINDOW)[None, :, None]
    )
    key_pos = (
        offset
        - WINDOW
        + jnp.arange(blocks)[:, None, None] * WINDOW
        + jnp.arange(3 * WINDOW)[None, None, :]
    )
    allowed = (jnp.abs(query_pos - key_pos) <= WINDOW) & (key_pos >= 0) & (key_pos < seq_total)
    scores = jnp.where(allowed[:, None], scores, -jnp.inf)
    sink_level = sink.reshape(1, heads_dev, 1, 1)
    row_peak = jnp.maximum(scores.max(-1, keepdims=True), sink_level)
    probabilities = jnp.exp(scores - row_peak)
    denominator = probabilities.sum(-1, keepdims=True) + jnp.exp(sink_level - row_peak)
    weights = (probabilities / denominator).astype(jnp.bfloat16)
    attended = jnp.einsum("nhqj,njd->nqhd", weights, value_band, preferred_element_type=jnp.float32)
    attended = attended.astype(jnp.bfloat16).reshape(tok_dev, heads_dev * HD)
    rows_dev = tok_dev // n_tp
    d_dev = w_down.shape[2]
    projected = lax.psum_scatter(
        jnp.dot(attended, w_out, preferred_element_type=jnp.float32),
        "tp",
        scatter_dimension=0,
        tiled=True,
    )
    mixed_rows = (stream.astype(jnp.float32) + projected).astype(jnp.bfloat16)
    whole_rows = lax.all_gather(mixed_rows, "tp", axis=0, tiled=True)
    wide_rows = whole_rows.astype(jnp.float32)
    scale_rows = lax.rsqrt(jnp.mean(wide_rows * wide_rows, axis=-1, keepdims=True) + NORM_EPS)
    normed = (wide_rows * scale_rows * gain.astype(jnp.float32)).astype(jnp.bfloat16)
    residual = lax.dynamic_slice_in_dim(wide_rows, tp_idx * d_dev, d_dev, 1)
    exp_dev = w_gate.shape[0]
    capacity = max(1, 2 * tok_dev * TOPK // (n_tp * EXPERTS))
    slot_count = EXPERTS * capacity
    blocked_routes = routes.reshape(n_tp, rows_dev, TOPK)
    destination = jax.vmap(lambda block_routes: slot_ids(block_routes, capacity))(blocked_routes)
    slot_select = destination[:, None, :] == jnp.arange(slot_count)[None, :, None]
    slot_select = slot_select.reshape(n_tp, slot_count, rows_dev, TOPK).astype(jnp.float32)
    dispatch_table = jnp.sum(slot_select, axis=-1).astype(jnp.bfloat16)
    combine_table = jnp.sum(slot_select * route_weights.reshape(n_tp, 1, rows_dev, TOPK), axis=-1)
    normed_blocks = normed.reshape(n_tp, rows_dev, D)
    own_table = lax.dynamic_index_in_dim(dispatch_table, tp_idx, 0, keepdims=False)
    own_rows = lax.dynamic_index_in_dim(normed_blocks, tp_idx, 0, keepdims=False)
    outgoing = jnp.dot(own_table, own_rows, preferred_element_type=jnp.float32).astype(jnp.bfloat16)
    arrived = lax.all_to_all(outgoing, "sp", split_axis=0, concat_axis=0, tiled=True)
    arrived = arrived.reshape(1, n_sp, exp_dev, capacity, D)
    piece_rows = lax.all_gather(arrived, "tp", axis=0, tiled=True)
    gate_act = jnp.einsum(
        "tsecd,efd->tsecf", piece_rows, w_gate, preferred_element_type=jnp.float32
    )
    up_act = jnp.einsum("tsecd,efd->tsecf", piece_rows, w_up, preferred_element_type=jnp.float32)
    hidden = (jax.nn.silu(gate_act) * up_act).astype(jnp.bfloat16)
    shared_gate_act = jnp.einsum(
        "td,fd->tf", normed, shared_gate, preferred_element_type=jnp.float32
    )
    shared_up_act = jnp.einsum("td,fd->tf", normed, shared_up, preferred_element_type=jnp.float32)
    shared_hidden = (jax.nn.silu(shared_gate_act) * shared_up_act).astype(jnp.bfloat16)
    shared_hidden = shared_hidden.reshape(1, 1, 1, tok_dev, shared_hidden.shape[1])
    expert_piece = lax.all_gather(hidden, "tp", axis=4, tiled=True)
    shared_piece = lax.all_gather(shared_hidden, "tp", axis=4, tiled=True)
    piece_width = expert_piece.shape[4]
    routed_total = jnp.einsum(
        "tsecf,efd->tsecd", expert_piece, w_down, preferred_element_type=jnp.float32
    )
    shared_total = jnp.dot(
        shared_piece.reshape(tok_dev, piece_width), shared_down, preferred_element_type=jnp.float32
    )
    returned = lax.all_to_all(
        routed_total.astype(jnp.bfloat16), "sp", split_axis=1, concat_axis=1, tiled=True
    )
    returned = returned.reshape(n_tp, slot_count, d_dev).astype(jnp.float32)
    routed = jnp.einsum("tmr,tmd->trd", combine_table, returned, precision=lax.Precision.HIGHEST)
    routed = routed.reshape(tok_dev, d_dev)
    return (residual + routed + shared_total).astype(jnp.bfloat16)


def solution(mesh):
    placed = (
        P("sp", "tp"),
        P("sp", None),
        P("sp", None),
        P("tp"),
        P("tp", None),
        P(("sp", "tp"), None),
        P(),
        P("sp", None),
        P("sp", None),
        P("sp", "tp", None),
        P("sp", "tp", None),
        P("sp", None, "tp"),
        P("tp", None),
        P("tp", None),
        P(None, "tp"),
    )
    return jax.shard_map(
        local, mesh=mesh, in_specs=placed, out_specs=P("sp", "tp"), check_vma=False
    )
```

profile of v0, /device:TPU:0, one launch (start us, length us, event | category | flops | bytes accessed | tf_op | source)
XLA Modules:
  0.0 317.8 jit_solution(6857469026317906916)
XLA Ops:
  6.5 1.1 constant_dynamic-slice_fusion
  7.6 0.1 fusion.32
  7.7 4.9 %collective-permute-start = (bf16[128,128]{1,0:T(8,128)(2,1)S(1)}, bf16[128,128]{1,0:T(8,128)(2,1)S(1)}, u32[]{:S(2)}, u32[]{:S(2)}) collective-permute-start(bf16[128,128]{1,0:T(8,128)(2,1)S(1)} %get-tuple-element.10), channel_id=1, source_target_pairs={{0,4},{4,8},{8,12},{12,16},{16,20},{20,24},{24,28},{1,5},{5,9},{9,... | collective-permute-start | bytes 98312 | tf_op jit(solution)/shard_map/ppermute | solution.py:23
  12.6 1.3 collective-permute-start.1
  13.9 0.1 iota_add_fusion
  14.0 0.1 fusion.37
  14.1 0.1 iota_add_fusion.1
  14.2 0.5 fusion.19
  14.6 1.1 reshape.199
  15.7 2.7 collective-permute-done.1
  18.4 0.1 pad_maximum_fusion.3
  18.5 0.1 copy.55
  18.6 0.1 copy.54
  18.8 0.1 copy.53
  18.9 0.4 fusion.41
  19.4 0.1 broadcast_maximum_fusion
  19.5 0.2 fusion.14
  19.7 0.1 exponential_add_fusion
  19.8 0.4 fusion.17
  20.2 0.1 copy.59
  20.4 1.8 fusion.27
  22.2 0.0 reduce-scatter.2.cloned.1.call-update
  22.2 0.0 all-gather.5.cloned.1.call-start
  22.3 32.5 %reduce-scatter.2.cloned.1.call-done = f32[64,2048]{1,0:T(8,128)} async-done(((f32[256,2048]{1,0:T(8,128)}), f32[64,2048]{1,0:T(8,128)}) %reduce-scatter.2.cloned.1.call-update) | async-done | bytes 524304 | tf_op jit(solution)/shard_map/reduce_scatter | solution.py:97
  54.7 1.8 add_convert_fusion
  56.5 0.0 all-gather.5.cloned.1.call-update
  56.5 0.0 all-gather.7.cloned.1.call-start
  56.6 0.1 copy.61
  56.7 0.1 eq.39
  56.9 0.1 eq.43
  57.0 0.1 copy.60
  57.2 2.4 reduce-window.6
  59.6 0.1 slice.53
  59.7 0.1 copy.63
  59.9 0.2 fusion.22
  60.0 0.1 reduce_sum.49
  60.2 0.1 copy.66
  60.3 0.1 mul.107
  60.4 1.3 convert_reduce_fusion
  61.7 11.7 %all-gather.5.cloned.1.call-done = bf16[256,2048]{1,0:T(8,128)(2,1)} async-done(((bf16[64,2048]{1,0:T(8,128)(2,1)}), bf16[256,2048]{1,0:T(8,128)(2,1)}) %all-gather.5.cloned.1.call-update) | async-done | bytes 1048592 | tf_op jit(solution)/shard_map/all_gather | solution.py:104
  73.4 1.5 multiply_reduce_fusion
  74.9 1.5 multiply_convert_fusion
  76.5 0.7 convolution_convert_fusion
  77.2 53.9 %all_to_all.14 = bf16[8,64,2048]{2,1,0:T(8,128)(2,1)S(1)} all-to-all(bf16[8,64,2048]{2,1,0:T(8,128)(2,1)S(1)} %bitcast.114), channel_id=1, replica_groups=mesh['sp'=8,'tp'=4] {'sp'}, dimensions={0} | all-to-all | bytes 4194304 | tf_op jit(solution)/shard_map/all_to_all | solution.py:122
  131.1 1.5 copy.68
  132.6 0.2 all-gather.9.cloned.1.call-start
  132.8 56.3 %all-gather.7.cloned.1.call-done = bf16[4,8,8,8,2048]{4,3,1,0,2:T(8,128)(2,1)} async-done(((bf16[1,8,8,8,2048]{4,3,1,0,2:T(8,128)(2,1)}), bf16[4,8,8,8,2048]{4,3,1,0,2:T(8,128)(2,1)}) %all-gather.7.cloned.1.call-update) | async-done | bytes 8388624 | tf_op jit(solution)/shard_map/all_gather | solution.py:124
  189.2 8.1 %fusion.4 = f32[8,4,8,8,256]{4,3,2,1,0:T(8,128)S(1)} fusion(bf16[4,8,8,8,2048]{4,3,1,0,2:T(8,128)(2,1)} %all-gather.7.cloned.1.call-done, bf16[8,256,2048]{2,1,0:T(8,128)(2,1)} %param.24), kind=kOutput, calls=%fused_computation.4 | convolution fusion | flops 2147483648 | bytes 18874368 | tf_op jit(solution)/shard_map/tsecd,efd->tsecf/dot_general | solution.py:125
  197.3 11.4 %fusion.6 = bf16[4,8,8,8,256]{4,3,1,0,2:T(8,128)(2,1)} fusion(f32[8,4,8,8,256]{4,3,2,1,0:T(8,128)S(1)} %fusion.4, bf16[4,8,8,8,2048]{4,3,1,0,2:T(8,128)(2,1)} %all-gather.7.cloned.1.call-done, bf16[8,256,2048]{2,1,0:T(8,128)(2,1)} %param.25), kind=kOutput, calls=%fused_computation.8 | convolution fusion | flops 2150629376 | bytes 19922944 | tf_op jit(solution)/shard_map/tsecd,efd->tsecf/dot_general | solution.py:128
  208.7 35.2 %all-gather.9.cloned.1.call-done = bf16[4,8,8,8,1024]{4,3,1,0,2:T(8,128)(2,1)} async-done(((bf16[4,8,8,8,256]{4,3,1,0,2:T(8,128)(2,1)}), bf16[4,8,8,8,1024]{4,3,1,0,2:T(8,128)(2,1)}) %all-gather.9.cloned.1.call-update) | async-done | bytes 4194320 | tf_op jit(solution)/shard_map/all_gather | solution.py:136
  243.8 7.0 %convert_bitcast_fusion = bf16[4,8,8,8,512]{4,3,1,0,2:T(8,128)(2,1)S(1)} fusion(bf16[4,8,8,8,1024]{4,3,1,0,2:T(8,128)(2,1)} %all-gather.9.cloned.1.call-done, bf16[8,1024,512]{2,1,0:T(8,128)(2,1)} %param.26), kind=kOutput, calls=%fused_computation.14 | convolution fusion | flops 2148532224 | bytes 14680064 | tf_op jit(solution)/shard_map/tsecf,efd->tsecd/dot_general | solution.py:139
  250.8 1.6 copy.69
  252.4 5.6 %all-to-all-start.1 = ((bf16[4,8,8,8,512]{4,3,0,2,1:T(8,128)(2,1)}), bf16[4,8,8,8,512]{4,3,0,2,1:T(8,128)(2,1)S(1)}, u32[]{:S(2)}, u32[]{:S(2)}) async-start(bf16[4,8,8,8,512]{4,3,0,2,1:T(8,128)(2,1)} %copy.69), calls=%async_computation.2 | async-start | bytes 4194304 | tf_op jit(solution)/shard_map/all_to_all | solution.py:145
  258.1 1.6 convert_element_type.61
  259.7 0.7 copy-done.7
  260.4 0.5 fusion.43
  260.8 0.5 fusion.16
  261.3 7.4 %all-gather = bf16[256,1024]{1,0:T(8,128)(2,1)} all-gather(bf16[256,256]{1,0:T(8,128)(2,1)S(1)} %fusion.16), channel_id=2, replica_groups=mesh['sp'=8,'tp'=4] {'tp'}, dimensions={1}, use_global_device_ids=true | all-gather | bytes 655360 | tf_op jit(solution)/shard_map/all_gather | solution.py:137
  268.7 38.0 %all-to-all-done.1 = bf16[4,8,8,8,512]{4,3,0,2,1:T(8,128)(2,1)S(1)} async-done(((bf16[4,8,8,8,512]{4,3,0,2,1:T(8,128)(2,1)}), bf16[4,8,8,8,512]{4,3,0,2,1:T(8,128)(2,1)S(1)}, u32[]{:S(2)}, u32[]{:S(2)}) %all-to-all-start.1) | async-done | bytes 2097184 | tf_op jit(solution)/shard_map/all_to_all | solution.py:145
  306.7 0.3 copy.70
  307.0 0.8 copy-done.6
  307.8 1.2 fusion.42
  308.9 1.1 bitcast_add_fusion
  310.1 1.1 fusion.15
  (44 shorter events, 0.2 us)
Async XLA Ops:
  6.5 13.8 %copy-start = (bf16[256,2048]{1,0:T(8,128)(2,1)S(1)}, bf16[256,2048]{1,0:T(8,128)(2,1)}, u32[]{:S(2)}) copy-start(bf16[256,2048]{1,0:T(8,128)(2,1)} %param.19) | copy-start | bytes 3145732
  6.5 48.2 %reduce-scatter.2.cloned.1.call-start = ((), (), s32[]{:S(2)}) async-start(), calls=%async_computation.3 | async-start | bytes 2621440 | tf_op jit(solution)/shard_map/reduce_scatter | solution.py:97
  6.5 12.9 %copy-start.13 = (f32[4]{0:T(128)S(1)}, f32[4]{0:T(128)}, u32[]{:S(2)}) copy-start(f32[4]{0:T(128)} %param.18) | copy-start | bytes 52
  7.7 8.0 %collective-permute-start = (bf16[128,128]{1,0:T(8,128)(2,1)S(1)}, bf16[128,128]{1,0:T(8,128)(2,1)S(1)}, u32[]{:S(2)}, u32[]{:S(2)}) collective-permute-start(bf16[128,128]{1,0:T(8,128)(2,1)S(1)} %get-tuple-element.10), channel_id=1, source_target_pairs={{0,4},{4,8},{8,12},{12,16},{16,20},{20,24},{24,28},{1,5},{5,9},{9,... | collective-permute-start | bytes 98312 | tf_op jit(solution)/shard_map/ppermute | solution.py:23
  12.6 5.8 %collective-permute-start.1 = (bf16[128,128]{1,0:T(8,128)(2,1)S(1)}, bf16[128,128]{1,0:T(8,128)(2,1)S(1)}, u32[]{:S(2)}, u32[]{:S(2)}) collective-permute-start(bf16[128,128]{1,0:T(8,128)(2,1)S(1)} %get-tuple-element.11), channel_id=1, source_target_pairs={{4,0},{8,4},{12,8},{16,12},{20,16},{24,20},{28,24},{5,1},{9,5},{13... | collective-permute-start | bytes 98312 | tf_op jit(solution)/shard_map/ppermute | solution.py:24
  20.4 34.4 %copy-start.9 = (bf16[64,2048]{1,0:T(8,128)(2,1)S(1)}, bf16[64,2048]{1,0:T(8,128)(2,1)}, u32[]{:S(2)}) copy-start(bf16[64,2048]{1,0:T(8,128)(2,1)} %param.20) | copy-start | bytes 786436
  22.2 34.4 %copy-start.10 = (s32[256,4]{0,1:T(4,128)S(1)}, s32[256,4]{0,1:T(4,128)}, u32[]{:S(2)}) copy-start(s32[256,4]{0,1:T(4,128)} %param.22) | copy-start | bytes 12292
  22.2 38.1 %copy-start.11 = (f32[256,4]{0,1:T(4,128)S(1)}, f32[256,4]{0,1:T(4,128)}, u32[]{:S(2)}) copy-start(f32[256,4]{0,1:T(4,128)} %param.23) | copy-start | bytes 12292
  22.2 38.2 %copy-start.12 = (bf16[2048]{0:T(1024)(128)(2,1)S(1)}, bf16[2048]{0:T(1024)(128)(2,1)}, u32[]{:S(2)}) copy-start(bf16[2048]{0:T(1024)(128)(2,1)} %param.21) | copy-start | bytes 12292
  22.2 51.2 %all-gather.5.cloned.1.call-start = ((), (), s32[]{:S(2)}) async-start(), calls=%async_computation.4 | async-start | bytes 1310720 | tf_op jit(solution)/shard_map/all_gather | solution.py:104
  56.5 132.6 %all-gather.7.cloned.1.call-start = ((), (), s32[]{:S(2)}) async-start(), calls=%async_computation.5 | async-start | bytes 10485760 | tf_op jit(solution)/shard_map/all_gather | solution.py:124
  76.5 54.6 %copy-start.3 = (bf16[256,2048]{1,0:T(8,128)(2,1)}, bf16[256,2048]{1,0:T(8,128)(2,1)S(1)}, u32[]{:S(2)}) copy-start(bf16[256,2048]{1,0:T(8,128)(2,1)S(1)} %multiply_convert_fusion) | copy-start | bytes 3145732
  132.6 111.2 %all-gather.9.cloned.1.call-start = ((), (), s32[]{:S(2)}) async-start(), calls=%async_computation.6 | async-start | bytes 5242880 | tf_op jit(solution)/shard_map/all_gather | solution.py:136
  252.4 5.6 %copy-start.2 = (bf16[256,2048]{1,0:T(8,128)(2,1)S(1)}, bf16[256,2048]{1,0:T(8,128)(2,1)}, u32[]{:S(2)}) copy-start(bf16[256,2048]{1,0:T(8,128)(2,1)} %all-gather.5.cloned.1.call-done) | copy-start | bytes 3145732
  252.4 54.3 %all-to-all-start.1 = ((bf16[4,8,8,8,512]{4,3,0,2,1:T(8,128)(2,1)}), bf16[4,8,8,8,512]{4,3,0,2,1:T(8,128)(2,1)S(1)}, u32[]{:S(2)}, u32[]{:S(2)}) async-start(bf16[4,8,8,8,512]{4,3,0,2,1:T(8,128)(2,1)} %copy.69), calls=%async_computation.2 | async-start | bytes 4194304 | tf_op jit(solution)/shard_map/all_to_all | solution.py:145
  258.1 1.6 copy-start.4
  258.1 2.3 copy-start.7
  258.1 2.8 copy-start.14
  306.7 1.0 copy-start.6
  307.8 2.3 copy-start.5
  307.8 2.3 copy-start.8
  307.8 3.5 %copy-start.1 = (bf16[256,2048]{1,0:T(8,128)(2,1)S(1)}, bf16[256,2048]{1,0:T(8,128)(2,1)}, u32[]{:S(2)}) copy-start(bf16[256,2048]{1,0:T(8,128)(2,1)} %param.19) | copy-start | bytes 3145732
Sparse Core Ops, SparseCore 0:
  22.3 32.3 reduce-scatter.1
  56.7 16.6 all-gather.4
  132.7 56.3 all-gather.6
  208.8 34.9 all-gather.8
where the time goes:
time: 318 us
  waiting for transfers between devices  176 us (55%)
  blocking collectives  61.2 us (19%)
  matrix products  33.1 us (10%)
  between operations  13.5 us (4%)
  other arithmetic  12.7 us (4%)
  starting transfers between devices  12.1 us (4%)
  local copies, waits for them, and re-layouts  8.65 us (3%)
    all_gather x1, waiting for transfers between devices, local(): piece_rows = lax.all_gather(arrived, 'tp', axis=0, tiled=True)  56.3 us
    all_to_all x1, blocking collectives, local(): lax.all_to_all(outgoing, 'sp', split_axis=0, concat_axis=0, tiled=True)  53.9 us
    all_to_all x1, waiting for transfers between devices, local(): lax.all_to_all(routed_total.astype(jnp.bfloat16), 'sp', split_axis=1, con...  38 us
    all_gather x1, waiting for transfers between devices, local(): expert_piece = lax.all_gather(hidden, 'tp', axis=4, tiled=True)  35.2 us
    reduce_scatter x1, waiting for transfers between devices, local(): lax.psum_scatter(jnp.dot(attended, w_out, preferred_element_type=jnp.floa...  32.5 us
    all_gather x1, waiting for transfers between devices, local(): whole_rows = lax.all_gather(mixed_rows, 'tp', axis=0, tiled=True)  11.7 us
    dot_general x1, matrix products, local(): jnp.einsum('tsecd,efd->tsecf', piece_rows, w_up, preferred_element_type=j...  11.4 us
    dot_general x1, matrix products, local(): jnp.einsum('tsecd,efd->tsecf', piece_rows, w_gate, preferred_element_type...  8.13 us
  transfers between devices with their start and end apart: 7, of which 6 were waited for; matrix products, arithmetic and copies ran while one was open for 3% of the time, Pallas kernels for 0%

commit v1 on v0

--- a/solution.py
+++ b/solution.py
@@ -133,7 +133,7 @@
     shared_up_act = jnp.einsum("td,fd->tf", normed, shared_up, preferred_element_type=jnp.float32)
     shared_hidden = (jax.nn.silu(shared_gate_act) * shared_up_act).astype(jnp.bfloat16)
     shared_hidden = shared_hidden.reshape(1, 1, 1, tok_dev, shared_hidden.shape[1])
-    expert_piece = lax.all_gather(hidden, "tp", axis=4, tiled=True)
+    expert_piece = jnp.concatenate(lax.all_gather(hidden, "tp"), axis=4)
     shared_piece = lax.all_gather(shared_hidden, "tp", axis=4, tiled=True)
     piece_width = expert_piece.shape[4]
     routed_total = jnp.einsum(

time: 318 us -> 319 us (level)
  no operation moved by 1% of the time
where the time goes in v1:
time: 319 us
  waiting for transfers between devices  176 us (55%)
  blocking collectives  61.2 us (19%)
  matrix products  31.9 us (10%)
  between operations  13.5 us (4%)
  other arithmetic  12.7 us (4%)
  starting transfers between devices  12.1 us (4%)
  local copies, waits for them, and re-layouts  11.4 us (4%)
    all_gather x1, waiting for transfers between devices, local(): piece_rows = lax.all_gather(arrived, 'tp', axis=0, tiled=True)  56.3 us
    all_to_all x1, blocking collectives, local(): lax.all_to_all(outgoing, 'sp', split_axis=0, concat_axis=0, tiled=True)  53.9 us
    all_to_all x1, waiting for transfers between devices, local(): lax.all_to_all(routed_total.astype(jnp.bfloat16), 'sp', split_axis=1, con...  38 us
    all_gather x1, waiting for transfers between devices, local(): expert_piece = jnp.concatenate(lax.all_gather(hidden, 'tp'), axis=4)  34.6 us
    reduce_scatter x1, waiting for transfers between devices, local(): lax.psum_scatter(jnp.dot(attended, w_out, preferred_element_type=jnp.floa...  32.5 us
    all_gather x1, waiting for transfers between devices, local(): whole_rows = lax.all_gather(mixed_rows, 'tp', axis=0, tiled=True)  11.7 us
    dot_general x1, matrix products, local(): jnp.einsum('tsecd,efd->tsecf', piece_rows, w_up, preferred_element_type=j...  11.4 us
    dot_general x1, matrix products, local(): jnp.einsum('tsecd,efd->tsecf', piece_rows, w_gate, preferred_element_type...  8.13 us
  transfers between devices with their start and end apart: 7, of which 6 were waited for; matrix products, arithmetic and copies ran while one was open for 3% of the time, Pallas kernels for 0%

profile of v1, /device:TPU:0, one launch (start us, length us, event | category | flops | bytes accessed | tf_op | source)
XLA Modules:
  0.0 318.7 jit_solution(9521204480455232224)
XLA Ops:
  6.5 1.1 constant_dynamic-slice_fusion
  7.6 0.1 fusion.32
  7.7 4.9 %collective-permute-start = (bf16[128,128]{1,0:T(8,128)(2,1)S(1)}, bf16[128,128]{1,0:T(8,128)(2,1)S(1)}, u32[]{:S(2)}, u32[]{:S(2)}) collective-permute-start(bf16[128,128]{1,0:T(8,128)(2,1)S(1)} %get-tuple-element.10), channel_id=1, source_target_pairs={{0,4},{4,8},{8,12},{12,16},{16,20},{20,24},{24,28},{1,5},{5,9},{9,... | collective-permute-start | bytes 98312 | tf_op jit(solution)/shard_map/ppermute | solution.py:23
  12.6 1.3 collective-permute-start.1
  13.9 0.1 iota_add_fusion
  14.0 0.1 fusion.37
  14.1 0.1 iota_add_fusion.1
  14.2 0.5 fusion.19
  14.6 1.1 reshape.208
  15.7 2.7 collective-permute-done.1
  18.4 0.1 pad_maximum_fusion.3
  18.5 0.1 copy.58
  18.6 0.1 copy.57
  18.8 0.1 copy.56
  18.9 0.4 fusion.41
  19.4 0.1 broadcast_maximum_fusion
  19.5 0.2 fusion.14
  19.7 0.1 exponential_add_fusion
  19.8 0.4 fusion.17
  20.2 0.1 copy.62
  20.4 1.8 fusion.27
  22.2 0.0 reduce-scatter.2.cloned.1.call-update
  22.2 0.0 all-gather.6.cloned.1.call-start
  22.3 32.5 %reduce-scatter.2.cloned.1.call-done = f32[64,2048]{1,0:T(8,128)} async-done(((f32[256,2048]{1,0:T(8,128)}), f32[64,2048]{1,0:T(8,128)}) %reduce-scatter.2.cloned.1.call-update) | async-done | bytes 524304 | tf_op jit(solution)/shard_map/reduce_scatter | solution.py:97
  54.7 1.8 add_convert_fusion
  56.5 0.0 all-gather.8.cloned.1.call-start
  56.6 0.1 copy.64
  56.7 0.1 eq.39
  56.9 0.1 eq.43
  57.0 0.1 copy.63
  57.2 2.4 reduce-window.6
  59.6 0.1 slice.53
  59.7 0.1 copy.66
  59.9 0.2 fusion.22
  60.0 0.1 reduce_sum.49
  60.2 0.1 copy.69
  60.3 0.1 mul.107
  60.4 1.3 convert_reduce_fusion
  61.7 11.7 %all-gather.6.cloned.1.call-done = bf16[256,2048]{1,0:T(8,128)(2,1)} async-done(((bf16[64,2048]{1,0:T(8,128)(2,1)}), bf16[256,2048]{1,0:T(8,128)(2,1)}) %all-gather.6.cloned.1.call-update) | async-done | bytes 1048592 | tf_op jit(solution)/shard_map/all_gather | solution.py:104
  73.4 1.5 multiply_reduce_fusion
  74.9 1.5 multiply_convert_fusion
  76.5 0.7 convolution_convert_fusion
  77.2 53.9 %all_to_all.14 = bf16[8,64,2048]{2,1,0:T(8,128)(2,1)S(1)} all-to-all(bf16[8,64,2048]{2,1,0:T(8,128)(2,1)S(1)} %bitcast.118), channel_id=1, replica_groups=mesh['sp'=8,'tp'=4] {'sp'}, dimensions={0} | all-to-all | bytes 4194304 | tf_op jit(solution)/shard_map/all_to_all | solution.py:122
  131.1 1.5 copy.71
  132.6 0.2 all-gather.10.cloned.1.call-start
  132.8 56.3 %all-gather.8.cloned.1.call-done = bf16[4,8,8,8,2048]{4,3,1,0,2:T(8,128)(2,1)} async-done(((bf16[1,8,8,8,2048]{4,3,1,0,2:T(8,128)(2,1)}), bf16[4,8,8,8,2048]{4,3,1,0,2:T(8,128)(2,1)}) %all-gather.8.cloned.1.call-update) | async-done | bytes 8388624 | tf_op jit(solution)/shard_map/all_gather | solution.py:124
  189.2 8.1 %fusion.4 = f32[8,4,8,8,256]{4,3,2,1,0:T(8,128)S(1)} fusion(bf16[4,8,8,8,2048]{4,3,1,0,2:T(8,128)(2,1)} %all-gather.8.cloned.1.call-done, bf16[8,256,2048]{2,1,0:T(8,128)(2,1)} %param.24), kind=kOutput, calls=%fused_computation.4 | convolution fusion | flops 2147483648 | bytes 18874368 | tf_op jit(solution)/shard_map/tsecd,efd->tsecf/dot_general | solution.py:125
  197.3 11.4 %fusion.6 = bf16[4,8,8,8,256]{4,3,1,0,2:T(8,128)(2,1)} fusion(f32[8,4,8,8,256]{4,3,2,1,0:T(8,128)S(1)} %fusion.4, bf16[4,8,8,8,2048]{4,3,1,0,2:T(8,128)(2,1)} %all-gather.8.cloned.1.call-done, bf16[8,256,2048]{2,1,0:T(8,128)(2,1)} %param.25), kind=kOutput, calls=%fused_computation.8 | convolution fusion | flops 2150629376 | bytes 19922944 | tf_op jit(solution)/shard_map/tsecd,efd->tsecf/dot_general | solution.py:128
  208.7 34.6 %all-gather.10.cloned.1.call-done = bf16[16,8,8,8,256]{4,3,1,0,2:T(8,128)(2,1)} async-done(((bf16[4,8,8,8,256]{4,3,1,0,2:T(8,128)(2,1)}), bf16[16,8,8,8,256]{4,3,1,0,2:T(8,128)(2,1)}) %all-gather.10.cloned.1.call-update) | async-done | bytes 4194320 | tf_op jit(solution)/shard_map/all_gather | solution.py:136
  243.3 2.7 copy.72
  246.0 5.8 %convert_bitcast_fusion = bf16[4,8,8,8,512]{4,3,1,0,2:T(8,128)(2,1)S(1)} fusion(bf16[4,8,8,8,1024]{4,3,1,0,2:T(8,128)(2,1)S(1)} %bitcast.122, bf16[8,1024,512]{2,1,0:T(8,128)(2,1)} %param.26), kind=kOutput, calls=%fused_computation.14 | convolution fusion | flops 2148532224 | bytes 14680064 | tf_op jit(solution)/shard_map/tsecf,efd->tsecd/dot_general | solution.py:139
  251.8 1.6 copy.73
  253.4 5.6 %all-to-all-start.1 = ((bf16[4,8,8,8,512]{4,3,0,2,1:T(8,128)(2,1)}), bf16[4,8,8,8,512]{4,3,0,2,1:T(8,128)(2,1)S(1)}, u32[]{:S(2)}, u32[]{:S(2)}) async-start(bf16[4,8,8,8,512]{4,3,0,2,1:T(8,128)(2,1)} %copy.73), calls=%async_computation.2 | async-start | bytes 4194304 | tf_op jit(solution)/shard_map/all_to_all | solution.py:145
  259.1 1.6 convert_element_type.61
  260.6 0.7 copy-done.7
  261.3 0.5 fusion.43
  261.8 0.5 fusion.16
  262.3 7.3 %all-gather.1 = bf16[256,1024]{1,0:T(8,128)(2,1)} all-gather(bf16[256,256]{1,0:T(8,128)(2,1)S(1)} %fusion.16), channel_id=3, replica_groups=mesh['sp'=8,'tp'=4] {'tp'}, dimensions={1}, use_global_device_ids=true | all-gather | bytes 655360 | tf_op jit(solution)/shard_map/all_gather | solution.py:137
  269.6 38.0 %all-to-all-done.1 = bf16[4,8,8,8,512]{4,3,0,2,1:T(8,128)(2,1)S(1)} async-done(((bf16[4,8,8,8,512]{4,3,0,2,1:T(8,128)(2,1)}), bf16[4,8,8,8,512]{4,3,0,2,1:T(8,128)(2,1)S(1)}, u32[]{:S(2)}, u32[]{:S(2)}) %all-to-all-start.1) | async-done | bytes 2097184 | tf_op jit(solution)/shard_map/all_to_all | solution.py:145
  307.7 0.3 copy.74
  307.9 0.8 copy-done.6
  308.7 1.2 fusion.42
  309.9 1.1 bitcast_add_fusion
  311.1 1.1 fusion.15
  (45 shorter events, 0.2 us)
Async XLA Ops:
  6.5 13.8 %copy-start = (bf16[256,2048]{1,0:T(8,128)(2,1)S(1)}, bf16[256,2048]{1,0:T(8,128)(2,1)}, u32[]{:S(2)}) copy-start(bf16[256,2048]{1,0:T(8,128)(2,1)} %param.19) | copy-start | bytes 3145732
  6.5 48.2 %reduce-scatter.2.cloned.1.call-start = ((), (), s32[]{:S(2)}) async-start(), calls=%async_computation.3 | async-start | bytes 2621440 | tf_op jit(solution)/shard_map/reduce_scatter | solution.py:97
  6.5 12.9 %copy-start.13 = (f32[4]{0:T(128)S(1)}, f32[4]{0:T(128)}, u32[]{:S(2)}) copy-start(f32[4]{0:T(128)} %param.18) | copy-start | bytes 52
  7.7 8.0 %collective-permute-start = (bf16[128,128]{1,0:T(8,128)(2,1)S(1)}, bf16[128,128]{1,0:T(8,128)(2,1)S(1)}, u32[]{:S(2)}, u32[]{:S(2)}) collective-permute-start(bf16[128,128]{1,0:T(8,128)(2,1)S(1)} %get-tuple-element.10), channel_id=1, source_target_pairs={{0,4},{4,8},{8,12},{12,16},{16,20},{20,24},{24,28},{1,5},{5,9},{9,... | collective-permute-start | bytes 98312 | tf_op jit(solution)/shard_map/ppermute | solution.py:23
  12.6 5.8 %collective-permute-start.1 = (bf16[128,128]{1,0:T(8,128)(2,1)S(1)}, bf16[128,128]{1,0:T(8,128)(2,1)S(1)}, u32[]{:S(2)}, u32[]{:S(2)}) collective-permute-start(bf16[128,128]{1,0:T(8,128)(2,1)S(1)} %get-tuple-element.11), channel_id=1, source_target_pairs={{4,0},{8,4},{12,8},{16,12},{20,16},{24,20},{28,24},{5,1},{9,5},{13... | collective-permute-start | bytes 98312 | tf_op jit(solution)/shard_map/ppermute | solution.py:24
  20.4 34.4 %copy-start.9 = (bf16[64,2048]{1,0:T(8,128)(2,1)S(1)}, bf16[64,2048]{1,0:T(8,128)(2,1)}, u32[]{:S(2)}) copy-start(bf16[64,2048]{1,0:T(8,128)(2,1)} %param.20) | copy-start | bytes 786436
  22.2 34.4 %copy-start.10 = (s32[256,4]{0,1:T(4,128)S(1)}, s32[256,4]{0,1:T(4,128)}, u32[]{:S(2)}) copy-start(s32[256,4]{0,1:T(4,128)} %param.22) | copy-start | bytes 12292
  22.2 38.1 %copy-start.11 = (f32[256,4]{0,1:T(4,128)S(1)}, f32[256,4]{0,1:T(4,128)}, u32[]{:S(2)}) copy-start(f32[256,4]{0,1:T(4,128)} %param.23) | copy-start | bytes 12292
  22.2 38.2 %copy-start.12 = (bf16[2048]{0:T(1024)(128)(2,1)S(1)}, bf16[2048]{0:T(1024)(128)(2,1)}, u32[]{:S(2)}) copy-start(bf16[2048]{0:T(1024)(128)(2,1)} %param.21) | copy-start | bytes 12292
  22.2 51.2 %all-gather.6.cloned.1.call-start = ((), (), s32[]{:S(2)}) async-start(), calls=%async_computation.4 | async-start | bytes 1310720 | tf_op jit(solution)/shard_map/all_gather | solution.py:104
  56.5 132.6 %all-gather.8.cloned.1.call-start = ((), (), s32[]{:S(2)}) async-start(), calls=%async_computation.5 | async-start | bytes 10485760 | tf_op jit(solution)/shard_map/all_gather | solution.py:124
  76.5 54.6 %copy-start.3 = (bf16[256,2048]{1,0:T(8,128)(2,1)}, bf16[256,2048]{1,0:T(8,128)(2,1)S(1)}, u32[]{:S(2)}) copy-start(bf16[256,2048]{1,0:T(8,128)(2,1)S(1)} %multiply_convert_fusion) | copy-start | bytes 3145732
  132.6 110.7 %all-gather.10.cloned.1.call-start = ((), (), s32[]{:S(2)}) async-start(), calls=%async_computation.6 | async-start | bytes 5242880 | tf_op jit(solution)/shard_map/all_gather | solution.py:136
  253.4 5.7 %copy-start.2 = (bf16[256,2048]{1,0:T(8,128)(2,1)S(1)}, bf16[256,2048]{1,0:T(8,128)(2,1)}, u32[]{:S(2)}) copy-start(bf16[256,2048]{1,0:T(8,128)(2,1)} %all-gather.6.cloned.1.call-done) | copy-start | bytes 3145732
  253.4 54.3 %all-to-all-start.1 = ((bf16[4,8,8,8,512]{4,3,0,2,1:T(8,128)(2,1)}), bf16[4,8,8,8,512]{4,3,0,2,1:T(8,128)(2,1)S(1)}, u32[]{:S(2)}, u32[]{:S(2)}) async-start(bf16[4,8,8,8,512]{4,3,0,2,1:T(8,128)(2,1)} %copy.73), calls=%async_computation.2 | async-start | bytes 4194304 | tf_op jit(solution)/shard_map/all_to_all | solution.py:145
  259.0 1.6 copy-start.4
  259.1 2.3 copy-start.7
  259.1 2.8 copy-start.14
  307.7 1.0 copy-start.6
  308.7 2.3 copy-start.5
  308.7 2.3 copy-start.8
  308.7 3.5 %copy-start.1 = (bf16[256,2048]{1,0:T(8,128)(2,1)S(1)}, bf16[256,2048]{1,0:T(8,128)(2,1)}, u32[]{:S(2)}) copy-start(bf16[256,2048]{1,0:T(8,128)(2,1)} %param.19) | copy-start | bytes 3145732
Sparse Core Ops, SparseCore 0:
  22.3 32.3 reduce-scatter.1
  56.7 16.6 all-gather.5
  132.7 56.3 all-gather.7
  208.8 34.4 all-gather.9
